TPU v7x, 512 devices: a whole 4x8x8 slice. The times are simulated.
512 devices in a mesh: sp: 64 (over z, y), tp: 8 (over x, core).
Axes of the slice: x: 4, y: 8, z: 8, core: 2. Of those that a mesh axis runs over, the one named last changes fastest.
Arguments:
- tokens: bfloat16 [24576, 2048], P('sp', 'tp'), may hold values from -60 to 60
- pre_gain: bfloat16 [2048], P('tp'), may hold values from 0.099609375 to 1.8984375
- w_query: bfloat16 [2048, 1024], P('sp', 'tp'), may hold values from -1 to 1
- w_key: bfloat16 [2048, 1024], P('sp', 'tp'), may hold values from -1 to 1
- w_value: bfloat16 [2048, 1024], P('sp', 'tp'), may hold values from -0.125 to 0.125
- w_pool: bfloat16 [2048, 1024], P('sp', 'tp'), may hold values from -0.125 to 0.125
- lambdas: float32 [8], P('tp'), may hold values from 0.3 to 0.8
- sub_gain: float32 [128], replicated, may hold values from 0.1 to 1.9
- group_weight: bfloat16 [8, 128, 128], P('tp'), may hold values from -0.5 to 0.5
- pool_scale: float32 [1024], P('tp'), may hold values from 0.1 to 1.9
- w_out: bfloat16 [2048, 2048], P('tp', 'sp'), may hold values from -0.125 to 0.125
Outputs:
- mixed_out: bfloat16 [24576, 2048], P(('sp', 'tp'))
All inputs are finite; a program needn't handle non-finite values.
Results may differ from a plain program's by a relative error of at most 0.015.
Values may be sent and summed in bfloat16 or wider, within the bound.
A program may use at most 128 MiB of HBM per device.

v0:
```python
import functools
import math

import jax
import jax.numpy as jnp
from jax import lax
from jax.experimental import pallas as pl
from jax.experimental.pallas import tpu as pltpu
from jax.sharding import PartitionSpec as P

MESH = pl.DeviceIdType.MESH
VMEM = pltpu.VMEM
EPSILON = 1e-06
NEG_LARGE = -1e30
F32, BF16 = jnp.float32, jnp.bfloat16
RIM = 16
DEPTH = 256
LEAD = 3
PARTS, EARLY = 8, 6


def grid_of(sp):
    ny = 2 ** ((sp.bit_length() - 1) // 2)
    return sp // ny, ny


def vspec(n):
    return [pl.BlockSpec(memory_space=VMEM)] * n


def sds(*shape, dtype=BF16):
    return jax.ShapeDtypeStruct(shape, dtype)


def call(kernel, ins, outs, scratch=(), cid=None, limit=40 << 20, name=None, flops=1 << 24, space=VMEM):
    params = dict(vmem_limit_bytes=limit)
    if cid is not None:
        params.update(collective_id=cid, has_side_effects=True)
    return pl.pallas_call(
        kernel,
        out_shape=tuple(outs),
        in_specs=[pl.BlockSpec(memory_space=space)] * len(ins),
        out_specs=tuple(vspec(len(outs))),
        scratch_shapes=list(scratch),
        compiler_params=pltpu.CompilerParams(**params),
        cost_estimate=pl.CostEstimate(flops=flops, bytes_accessed=1 << 20, transcendentals=0),
        name=name,
    )(*ins)


def rcopy(src, dst, ssem, rsem, dev):
    return pltpu.make_async_remote_copy(
        src_ref=src, dst_ref=dst, send_sem=ssem, recv_sem=rsem, device_id=dev, device_id_type=MESH
    )


def greet(peers):
    barrier = pltpu.get_barrier_semaphore()
    for dev in peers:
        pl.semaphore_signal(barrier, inc=1, device_id=dev, device_id_type=MESH)
    pl.semaphore_wait(barrier, len(peers))


def hops(n, direction, sub):
    return n // 2 if (direction + sub) % 2 == 0 else (n - 1) // 2


class Ring:
    def __init__(self, n, me, dev, piece, subs, ssem, rsem):
        self.n, self.me, self.dev, self.piece, self.subs = n, me, dev, piece, subs
        self.ssem, self.rsem = ssem, rsem
        self.steps = n // 2

    def copy(self, d, sub, k):
        sign = 1 if d == 0 else -1
        block = (self.me - sign * k) % self.n
        ref = self.piece(block, sub)
        return rcopy(
            ref, ref, self.ssem.at[d, sub, k], self.rsem.at[d, sub, k], self.dev((self.me + sign) % self.n)
        )

    def step(self, k, subs=None, landed=None):
        for sub in subs if subs is not None else range(self.subs):
            for d in range(2):
                if k > 0 and k - 1 < hops(self.n, d, sub):
                    self.copy(d, sub, k - 1).wait_recv()
                    if landed is not None:
                        landed((self.me + (k if d else -k)) % self.n, sub)
                if k < hops(self.n, d, sub):
                    self.copy(d, sub, k).start()

    def finish(self):
        for k in range(self.steps):
            for sub in range(self.subs):
                for d in range(2):
                    if k < hops(self.n, d, sub):
                        self.copy(d, sub, k).wait_send()


def ring_sems(n, subs):
    return [pltpu.SemaphoreType.DMA((2, subs, max(n // 2, 1))), pltpu.SemaphoreType.DMA((2, subs, max(n // 2, 1)))]


class Shared:
    def __init__(self, nx, own, buf, subs, size, rs, rr, ps, pr):
        s, t = lax.axis_index("sp"), lax.axis_index("tp")
        x, c = t // 2, t % 2
        self.nx, self.x, self.c, self.t = nx, x, c, t
        self.buf, self.ps, self.pr, self.own = buf, ps, pr, own
        self.partner = (s, x * 2 + 1 - c)
        self.peers = [(s, ((x + d) % nx) * 2 + c) for d in ((1, nx - 1) if nx > 1 else ())] + [self.partner]
        self.piece = lambda b, i: buf.at[2 * b + c, i * size : (i + 1) * size]
        self.ring = Ring(nx, x, lambda i: (s, 2 * i + c), self.piece, subs, rs, rr)
        self.subs = subs
        self.relays = []

    def relay(self, block, sub):
        ref = self.piece(block, sub)
        at = len(self.relays)
        copy = rcopy(ref, ref, self.ps.at[at], self.pr.at[at], self.partner)
        copy.start()
        self.relays.append(copy)

    def start(self):
        self.buf[self.t] = self.own[...]
        self.ring.step(0)
        self.direct = rcopy(
            self.own, self.buf.at[self.t], self.ps.at[self.subs * self.nx], self.pr.at[self.subs * self.nx], self.partner
        )
        self.direct.start()

    def step(self, k, subs):
        if k <= self.ring.steps:
            self.ring.step(k, subs, self.relay)

    def finish(self):
        for copy in self.relays + [self.direct]:
            copy.wait_recv()
        for copy in self.relays + [self.direct]:
            copy.wait_send()
        self.ring.finish()


def shared_sems(nx, subs):
    dma = pltpu.SemaphoreType.DMA
    return ring_sems(nx, subs) + [dma((subs * nx + 1,)), dma((subs * nx + 1,))]


def gather_kernel(nz, ny, nx, tin_ref, gain_ref, wq_ref, wk_ref, wv_ref, wp_ref, wo_ref, tok_full, w_full, tok_ref, w_ref, gain, ins, ts, tr, ys, yr, zs, zr, as_, ar, bs, br):
    s, t = lax.axis_index("sp"), lax.axis_index("tp")
    z, y, x, c = s // ny, s % ny, t // 2, t % 2
    half = w_ref.shape[0] // 2
    rows = tin_ref.shape[0]
    loads = [pltpu.make_async_copy(tin_ref, tok_ref.at[0:rows], ins.at[0]), pltpu.make_async_copy(gain_ref, gain, ins.at[1])]
    at = 0
    for i, ref in enumerate((wq_ref, wk_ref, wv_ref, wp_ref, wo_ref)):
        loads.append(pltpu.make_async_copy(ref, w_ref.at[:, at : at + ref.shape[1]], ins.at[2 + i]))
        at += ref.shape[1]
    for load in loads:
        load.start()
    loads[1].wait()
    tok_ref[rows:] = jnp.broadcast_to(gain[...], (16, gain.shape[1]))
    partner = (s, x * 2 + 1 - c)
    across = [(s, ((x + d) % nx) * 2 + c) for d in range(1, nx)]
    along_y = [(z * ny + (y + d) % ny, t) for d in range(1, ny)]
    along_z = [(((z + d) % nz) * ny + y, t) for d in range(1, nz)]
    greet([partner] + across + along_y + along_z)
    for i, load in enumerate(loads):
        if i != 1:
            load.wait()

    ysends = [
        rcopy(w_ref.at[0:half], w_full.at[z, y, 0], ys.at[d], yr.at[d], along_y[d]) for d in range(ny - 1)
    ]
    zsends = [
        rcopy(w_ref.at[half:], w_full.at[z, y, 1], zs.at[d], zr.at[d], along_z[d]) for d in range(nz - 1)
    ]
    tsends = [rcopy(tok_ref, tok_full.at[t], ts.at[d], tr.at[d], across[d]) for d in range(nx - 1)]
    tsends.append(rcopy(tok_ref, tok_full.at[t], ts.at[nx - 1], tr.at[nx - 1], partner))
    for copy in ysends + zsends + tsends:
        copy.start()
    w_full[z, y, 0] = w_ref[0:half]
    w_full[z, y, 1] = w_ref[half:]
    tok_full[t] = tok_ref[...]

    def piece_a(block, sub):
        return w_full.at[block, sub * (ny // 2) : (sub + 1) * (ny // 2), 0]

    def piece_b(block, sub):
        return w_full.at[sub * (nz // 2) : (sub + 1) * (nz // 2), block, 1]

    ring_a = Ring(nz, z, lambda i: (i * ny + y, t), piece_a, 2, as_, ar)
    ring_b = Ring(ny, y, lambda i: (z * ny + i, t), piece_b, 2, bs, br)
    for copy in ysends:
        copy.wait_recv()
    ring_a.step(0)
    for copy in zsends:
        copy.wait_recv()
    ring_b.step(0)
    relays = []
    for k in range(1, max(ring_a.steps, ring_b.steps) + 1):
        if k <= ring_a.steps:
            ring_a.step(k)
        if k <= ring_b.steps:
            ring_b.step(k)
        if k == 1:
            for d in range(nx - 1):
                tsends[d].wait_recv()
                source = ((x - 1 - d) % nx) * 2 + c
                relays.append(
                    rcopy(tok_full.at[source], tok_full.at[source], ts.at[nx + d], tr.at[nx + d], partner)
                )
                relays[-1].start()
    tsends[-1].wait_recv()
    for copy in relays:
        copy.wait_recv()
    for copy in ysends + zsends + tsends + relays:
        copy.wait_send()
    ring_a.finish()
    ring_b.finish()


def project_kernel(tp, tok_ref, w_ref, qt_ref, k_ref, vt_ref, pool_ref, early, late, scaled, sq):
    rows, part = qt_ref.shape[1], tok_ref.shape[2]
    early[...] = w_ref[0 : early.shape[0], 512:]
    late[...] = w_ref[early.shape[0] :, 512:]
    sq[...] = jnp.zeros_like(sq)
    for t in range(tp):
        x = tok_ref[t, 0:rows].astype(F32)
        gain = tok_ref[t, rows : rows + 1].astype(F32)
        squares = x * x
        for i in range(part // 128):
            sq[...] += squares[:, i * 128 : (i + 1) * 128]
        scaled[:, t * part : (t + 1) * part] = (x * gain).astype(BF16)
    inverse = lax.rsqrt(jnp.sum(sq[...], axis=1, keepdims=True) / (tp * part) + EPSILON)

    def project(at):
        out = jnp.dot(scaled[...], w_ref[:, at * 128 : at * 128 + 256], preferred_element_type=F32) * inverse
        return out[:, 0:128].astype(BF16), out[:, 128:256].astype(BF16)

    q, k = project(0)
    qt_ref[...] = jnp.transpose(q.astype(F32)).astype(BF16)
    k_ref[...] = k
    v, p = project(2)
    vt_ref[...] = jnp.transpose(v.astype(F32)).astype(BF16)
    pool_ref[...] = p


def attend_kernel(
    nz, ny, nx, scale, q_ref, k_ref, v_ref, p_ref, wo_ref, q_all, k_all, v_all, halo, wo_all, acc_ref, st_ref,
    qz_ref, sum_ref, zs, zr, ys, yr, xs, xr, ps, pr, hs, hr,
):
    s, t = lax.axis_index("sp"), lax.axis_index("tp")
    z, y = s // ny, s % ny
    sp = nz * ny
    dev_z = lambda i: (i * ny + y, t)
    dev_y = lambda i: (z * ny + i, t)
    rows = p_ref.shape[0]
    nxt, prv = ((s + 1) % sp, t), ((s + sp - 1) % sp, t)
    shared = Shared(nx, wo_ref, wo_all, EARLY, wo_ref.shape[0] // EARLY, xs, xr, ps, pr)
    near = [dev_z((z + 1) % nz), dev_z((z + nz - 1) % nz), dev_y((y + 1) % ny), dev_y((y + ny - 1) % ny)]
    greet(near + [nxt, prv] + shared.peers)
    q_all[y] = q_ref[...]
    k_all[z] = k_ref[...]
    v_all[z] = v_ref[...]
    half = q_ref.shape[0] // 2
    ring_y = Ring(ny, y, dev_y, lambda b, i: q_all.at[b, i * half : (i + 1) * half], 2, ys, yr)
    ring_z = Ring(nz, z, dev_z, lambda b, i: (k_all if i == 0 else v_all).at[b], 2, zs, zr)
    ring_y.step(0)
    ring_z.step(0)
    shared.start()
    hcopy = rcopy(p_ref.at[rows - RIM :], halo, hs, hr, nxt)
    hcopy.start()

    lanes = 2 * rows
    width = min(256, rows)
    vd = v_all.shape[1]
    factor = scale / math.log(2.0)

    def positions(yq, at, wide):
        lane = lax.broadcasted_iota(jnp.int32, (1, wide), 1) + at
        return jnp.where(lane >= rows, lane - rows, lane) + (z * ny + yq) * rows

    def begin(yq):
        qt = q_all[yq]
        low = lax.broadcasted_iota(jnp.int32, qt.shape, 0) < half
        zero = jnp.zeros_like(qt)
        qz_ref[yq, :, 0:rows] = jnp.where(low, qt, zero)
        qz_ref[yq, :, rows:] = jnp.where(low, zero, qt)
        acc_ref[yq] = jnp.zeros((vd, lanes), F32)
        sum_ref[yq] = jnp.zeros((8, lanes), F32)
        few = min(128, rows)
        source = jnp.where(yq >= y, z, jnp.maximum(z - 1, 0))
        sc = jnp.dot(k_all[source, 0:few], qz_ref[yq], preferred_element_type=F32)
        kpos = (source * ny + y) * rows + lax.broadcasted_iota(jnp.int32, (few, 1), 0)
        bar = jnp.max(jnp.where(kpos <= positions(yq, 0, lanes), sc, NEG_LARGE), axis=0, keepdims=True)
        st_ref[yq, 0:1] = bar
        st_ref[yq, 1:2] = bar * factor

    def tiles(yq, blocks, mask=None):
        keys = jnp.concatenate([k_all[b] for b in blocks], axis=0)
        vals = jnp.concatenate([v_all[b] for b in blocks], axis=1)
        depth = rows if len(blocks) == 1 else min(DEPTH, rows)
        work = [(at, low) for at in range(0, lanes, width) for low in range(0, keys.shape[0], depth)]

        def scores(item):
            at, low = item
            return jnp.dot(keys[low : low + depth], qz_ref[yq, :, at : at + width], preferred_element_type=F32)

        ahead = [scores(item) for item in work[:LEAD]]
        total, gain = None, None
        for i, (at, low) in enumerate(work):
            sc = ahead.pop(0)
            if i + LEAD < len(work):
                ahead.append(scores(work[i + LEAD]))
            cols = slice(at, at + width)
            expo = jnp.exp2(sc * factor - st_ref[yq, 1:2, cols])
            if mask is not None:
                expo = jnp.where(mask(at)[low : low + depth], expo, 0.0)
            part = jnp.sum(expo.reshape(depth // 8, 8, width), axis=0)
            total = part if low == 0 else total + part
            term = jnp.dot(vals[:, low : low + depth], expo.astype(BF16), preferred_element_type=F32)
            gain = term if low == 0 else gain + term
            if low + depth == keys.shape[0]:
                sum_ref[yq, :, cols] += total
                acc_ref[yq, :, cols] += gain

    def at_distance(j, yq):
        below = z >= j
        above = jnp.logical_and(z + j >= nz, 2 * j < nz)

        @pl.when(jnp.logical_and(below, above))
        def _():
            tiles(yq, [lax.rem(z + nz - j, nz), lax.rem(z + j, nz)])

        @pl.when(jnp.logical_xor(below, above))
        def _():
            tiles(yq, [lax.rem(jnp.where(below, z + nz - j, z + j), nz)])

    def query_block(i):
        away = (i + 1) // 2
        return lax.rem(y + jnp.where(i % 2 == 1, away, ny - away), ny)

    def first_visits(first, last):
        def visit(i, carry):
            yq = query_block(i)

            @pl.when(i > 0)
            def _():
                begin(yq)

                @pl.when(yq > y)
                def _():
                    tiles(yq, [z])

            at_distance(1, yq)
            return carry

        if first < last:
            lax.fori_loop(first, last, visit, 0)

    def later_visits(j):
        def visit(i, carry):
            at_distance(j, query_block(i))
            return carry

        lax.fori_loop(0, ny, visit, 0)

    begin(y)
    kpos = (z * ny + y) * rows + lax.broadcasted_iota(jnp.int32, (rows, 1), 0)
    tiles(y, [z], lambda at: kpos <= positions(y, at, width))
    sy, sz = ring_y.steps, ring_z.steps
    for k in range(1, min(sy, 2) + 1):
        ring_y.step(k)
    ring_z.step(1)
    here = min(ny, 2 * min(sy, 2) + 1)
    first_visits(0, min(3, here))
    if sy >= 3:
        ring_y.step(3)
    first_visits(3, here)
    if sz >= 2:
        ring_z.step(2)
    if sy >= 4:
        ring_y.step(4)
    shared.step(1, range(EARLY // 2))
    first_visits(here, ny)
    for j in range(2, sz + 1):
        if j < sz:
            ring_z.step(j + 1)
        if j + 1 == sz:
            shared.step(1, range(EARLY // 2, EARLY))
        later_visits(j)
    if sz < 3:
        shared.step(1, range(EARLY // 2, EARLY))
    shared.step(2, range(EARLY))
    for b in range(ny):
        st_ref[b, 1:2] = jnp.sum(sum_ref[b], axis=0, keepdims=True)
    hcopy.wait_recv()
    hcopy.wait_send()
    ring_z.finish()
    ring_y.finish()
    shared.finish()


def repair_kernel(ny, scale, q_all, k_all, v_all, acc_in, st_in, acc_ref, st_ref, qz_ref):
    s = lax.axis_index("sp")
    z, y = s // ny, s % ny
    rows = q_all.shape[2]
    half = q_all.shape[1] // 2
    lanes = 2 * rows
    factor = scale / math.log(2.0)
    calm = jnp.max(st_in[:, 1:2]) < 2.0**80

    @pl.when(calm)
    def _():
        acc_ref[...] = acc_in[...]
        st_ref[:, 0:2] = st_in[:, 0:2]

    @pl.when(jnp.logical_not(calm))
    def _():
        def slow(yq, carry):
            qt = q_all[yq]
            low = lax.broadcasted_iota(jnp.int32, qt.shape, 0) < half
            zero = jnp.zeros_like(qt)
            qz_ref[:, 0:rows] = jnp.where(low, qt, zero)
            qz_ref[:, rows:] = jnp.where(low, zero, qt)
            acc_ref[yq] = jnp.zeros((acc_ref.shape[1], lanes), F32)
            st_ref[yq, 0:1] = jnp.full((1, lanes), NEG_LARGE, F32)
            st_ref[yq, 1:2] = jnp.zeros((1, lanes), F32)

            def block(b, carry):
                kpos = (b * ny + y) * rows + lax.broadcasted_iota(jnp.int32, (rows, 1), 0)

                def group(g, carry):
                    at = pl.multiple_of(g * 128, 128)
                    cols = pl.ds(at, 128)
                    lane = lax.broadcasted_iota(jnp.int32, (1, 128), 1) + at
                    qpos = jnp.where(lane >= rows, lane - rows, lane) + (z * ny + yq) * rows
                    allowed = kpos <= qpos
                    sc = jnp.dot(k_all[b], qz_ref[:, cols], preferred_element_type=F32)
                    sc = jnp.where(allowed, sc, NEG_LARGE)
                    old = st_ref[yq, 0:1, cols]
                    new = jnp.maximum(old, jnp.max(sc, axis=0, keepdims=True))
                    expo = jnp.where(allowed, jnp.exp2((sc - new) * factor), 0.0)
                    shrink = jnp.exp2((old - new) * factor)
                    st_ref[yq, 0:1, cols] = new
                    st_ref[yq, 1:2, cols] = st_ref[yq, 1:2, cols] * shrink + jnp.sum(expo, axis=0, keepdims=True)
                    acc_ref[yq, :, cols] = acc_ref[yq, :, cols] * shrink + jnp.dot(
                        v_all[b], expo.astype(BF16), preferred_element_type=F32
                    )
                    return carry

                return lax.fori_loop(0, lanes // 128, group, carry)

            return lax.fori_loop(0, z + 1, block, carry)

        lax.fori_loop(0, ny, slow, 0)


def finish_kernel(
    ny, nx, scale, acc_ref, st_ref, lam_ref, gain_ref, p_ref, halo, gw_ref, ps_ref, wo_ref, late_ref, out_ref,
    mix, branch, wo_late, wbuf, sbuf, wland, sland, lands, ws, wr, ss, sr, xs, xr, ps, pr, os, or_,
):
    s, t = lax.axis_index("sp"), lax.axis_index("tp")
    z, y = s // ny, s % ny
    tp = 2 * nx
    rows, head = p_ref.shape
    orows = out_ref.shape[0]
    factor = scale / math.log(2.0)
    dev = lambda i: (z * ny + i % ny, t)
    shared = Shared(nx, late_ref, wo_late, PARTS - EARLY, late_ref.shape[0] // (PARTS - EARLY), xs, xr, ps, pr)
    others = [(s, (t + d) % tp) for d in range(1, tp)]
    greet([dev(y + 1), dev(y + ny - 1)] + others)

    def pooled():
        here = p_ref[...].astype(F32)
        rim = jnp.where(s > 0, halo[...].astype(F32), 0.0)
        total = jnp.concatenate([rim, here], axis=0)
        slot = t % 4
        for i in range(4):
            more = total + pltpu.roll(total, 1 << i, 0)
            total = jnp.where(i <= slot, more, total)
        span = jnp.where(slot == 0, 2, jnp.where(slot == 1, 4, jnp.where(slot == 2, 8, 16)))
        pos = s * rows + lax.broadcasted_iota(jnp.int32, (rows, 1), 0)
        count = jnp.minimum(pos + 1, span).astype(F32)
        differ = (total[RIM:] / count - here).astype(BF16)
        return (jnp.dot(differ, gw_ref[0], preferred_element_type=F32) * ps_ref[...]).astype(BF16)

    def own(block, m):
        cols = slice(m * rows, (m + 1) * rows)
        return acc_ref[block, :, cols], st_ref[block, 0:1, cols], st_ref[block, 1:2, cols]

    def joined(a, b):
        top = jnp.maximum(a[1], b[1])
        fa, fb = jnp.exp2((a[1] - top) * factor), jnp.exp2((b[1] - top) * factor)
        return a[0] * fa + b[0] * fb, top, a[2] * fa + b[2] * fb

    def landed(d, m, k):
        return wland[d, m, k].astype(F32), sland[d, m, k, 0:1], sland[d, m, k, 1:2]

    def copies(d, m, k):
        to = dev(y + (1 if d == 0 else ny - 1))
        return [
            rcopy(wbuf.at[d, m, k], wland.at[d, m, k], ws.at[d, m, k], wr.at[d, m, k], to),
            rcopy(sbuf.at[d, m, k], sland.at[d, m, k], ss.at[d, m, k], sr.at[d, m, k], to),
        ]

    for k in range(ny // 2):
        for m in range(2):
            for d in range(2):
                n = hops(ny, d, m)
                if k >= n:
                    continue
                sign = 1 if d == 0 else -1
                block = (y + sign * (n - k)) % ny
                state = own(block, m)
                if k > 0:
                    for copy in copies(d, m, k - 1):
                        copy.wait_recv()
                    state = joined(state, landed(d, m, k - 1))
                wbuf[d, m, k] = state[0].astype(BF16)
                sbuf[d, m, k, 0:1] = state[1]
                sbuf[d, m, k, 1:2] = state[2]
                for copy in copies(d, m, k):
                    copy.start()
        if k == 0:
            shared.start()
            branch[:, head:] = pooled()
        if k == min(2, ny // 2 - 1):
            shared.step(1, range(PARTS - EARLY))
    for m in range(2):
        state = own(y, m)
        for d in range(2):
            n = hops(ny, d, m)
            if n > 0:
                for copy in copies(d, m, n - 1):
                    copy.wait_recv()
                state = joined(state, landed(d, m, n - 1))
        if m == 0:
            mix[...] = state[0] / state[2]
        else:
            mix[...] = mix[...] - lam_ref[0:1, 0:1] * state[0] / state[2]
    mixed = mix[...]
    mean = jnp.mean(mixed * mixed, axis=0, keepdims=True)
    normed = jnp.transpose(mixed * lax.rsqrt(mean + EPSILON)) * gain_ref[...]
    branch[:, 0:head] = normed.astype(BF16)

    outs = []
    for d in range(1, tp):
        at = pl.multiple_of(((t + d) % tp) * orows, 16)
        outs.append(rcopy(branch.at[pl.ds(at, orows)], lands.at[t], os.at[d - 1], or_.at[d - 1], others[d - 1]))
        outs[-1].start()
    lands[t] = branch[pl.ds(pl.multiple_of(t * orows, 16), orows)]
    shared.step(2, range(PARTS - EARLY))
    shared.finish()
    for copy in outs:
        copy.wait_recv()
    at = 0
    for ref in (wo_ref, wo_late):
        step = math.gcd(512, ref.shape[1])
        for low in range(0, ref.shape[1], step):
            total = None
            for i in range(tp):
                term = lax.dot_general(
                    lands[i], ref[i, low : low + step], (((1,), (1,)), ((), ())), preferred_element_type=F32
                )
                total = term if total is None else total + term
            out_ref[:, at : at + step] = total.astype(BF16)
            at += step
    for copy in outs:
        copy.wait_send()
    for k in range(ny // 2):
        for m in range(2):
            for d in range(2):
                if k < hops(ny, d, m):
                    for copy in copies(d, m, k):
                        copy.wait_send()


def local(sp, tp, tokens, pre_gain, w_query, w_key, w_value, w_pool, lambdas, sub_gain, group_weight, pool_scale, w_out):
    nz, ny = grid_of(sp)
    nx = tp // 2
    rows, part = tokens.shape
    wrows = w_query.shape[0]
    head = w_value.shape[1]
    qd = w_query.shape[1]
    whole = 3 * qd + 3 * head
    ncols = sp * w_out.shape[1]
    early = ncols // PARTS * EARLY
    scale = 1.0 / math.sqrt(qd // 2)
    dma = pltpu.SemaphoreType.DMA
    tok_full, w_full = call(
        functools.partial(gather_kernel, nz, ny, nx),
        [
            pltpu.with_memory_space_constraint(a, pltpu.HBM)
            for a in (tokens, pre_gain.reshape(1, part), w_query, w_key, w_value, w_pool, w_out.T)
        ],
        (sds(tp, rows + 16, part), sds(nz, ny, 2, wrows // 2, whole)),
        [VMEM((rows + 16, part), BF16), VMEM((wrows, whole), BF16), VMEM((1, part), BF16), dma((7,))]
        + [dma((2 * nx,)), dma((2 * nx,)), dma((ny,)), dma((ny,)), dma((nz,)), dma((nz,))]
        + ring_sems(nz, 2)
        + ring_sems(ny, 2),
        cid=0,
        space=pltpu.HBM,
        name="gather",
    )
    qt, k, vt, pool, wo_early, wo_late = call(
        functools.partial(project_kernel, tp),
        (tok_full, w_full.reshape(sp * wrows, whole)),
        (sds(qd, rows), sds(rows, qd), sds(head, rows), sds(rows, head), sds(early, 2 * head), sds(ncols - early, 2 * head)),
        [VMEM((rows, tp * part), BF16), VMEM((rows, 128), F32)],
        name="project",
    )
    totals = (sds(ny, head, 2 * rows, dtype=F32), sds(ny, 8, 2 * rows, dtype=F32))
    q_all, k_all, v_all, halo, wo_all, acc, st = call(
        functools.partial(attend_kernel, nz, ny, nx, scale),
        (qt, k, vt, pool, wo_early),
        (sds(ny, qd, rows), sds(nz, rows, qd), sds(nz, head, rows), sds(RIM, head), sds(tp, early, 2 * head))
        + totals,
        [VMEM((ny, qd, 2 * rows), BF16), VMEM((ny, 8, 2 * rows), F32)]
        + ring_sems(nz, 2) + ring_sems(ny, 2) + shared_sems(nx, EARLY) + [dma, dma],
        cid=1,
        name="attend",
    )
    acc, st = call(
        functools.partial(repair_kernel, ny, scale),
        (q_all, k_all, v_all, acc, st),
        totals,
        [VMEM((qd, 2 * rows), BF16)],
        name="repair",
    )
    half = ny // 2
    orows = rows // tp
    (out,) = call(
        functools.partial(finish_kernel, ny, nx, scale),
        (
            acc,
            st,
            jnp.broadcast_to(lambdas.reshape(1, 1), (8, 128)),
            sub_gain.reshape(1, head),
            pool,
            halo,
            group_weight,
            pool_scale.reshape(1, head),
            wo_all,
            wo_late,
        ),
        (sds(orows, ncols),),
        [
            VMEM((head, rows), F32),
            VMEM((rows, 2 * head), BF16),
            VMEM((tp, ncols - early, 2 * head), BF16),
            VMEM((2, 2, half, head, rows), BF16),
            VMEM((2, 2, half, 8, rows), F32),
            VMEM((2, 2, half, head, rows), BF16),
            VMEM((2, 2, half, 8, rows), F32),
            VMEM((tp, orows, 2 * head), BF16),
        ]
        + [dma((2, 2, half))] * 4
        + shared_sems(nx, PARTS - EARLY)
        + [dma((tp,))] * 2,
        cid=2,
        name="finish",
    )
    return out


def solution(mesh):
    placed = (
        P("sp", "tp"),
        P("tp"),
        P("sp", "tp"),
        P("sp", "tp"),
        P("sp", "tp"),
        P("sp", "tp"),
        P("tp"),
        P(),
        P("tp", None, None),
        P("tp"),
        P("tp", "sp"),
    )
    body = functools.partial(local, mesh.shape["sp"], mesh.shape["tp"])
    return jax.shard_map(body, mesh=mesh, in_specs=placed, out_specs=P(("sp", "tp"), None), check_vma=False)
```

profile of v0, /device:TPU:449, one launch (start us, length us, event | category | flops | bytes accessed | tf_op | source)
XLA Modules:
  0.0 273.1 jit_solution(13128426749920821051)
XLA Ops:
  0.0 1.2 reshape.14.gain_ref
  1.2 32.9 %gather.1 = (bf16[8,400,256]{2,1,0:T(8,128)(2,1)S(1)}, bf16[8,8,2,16,768]{4,3,2,1,0:T(8,128)(2,1)S(1)}) custom-call(bf16[384,256]{1,0:T(8,128)(2,1)} %tin_ref.1, bf16[1,256]{1,0:T(2,128)(2,1)} %reshape.14.gain_ref, bf16[32,128]{1,0:T(8,128)(2,1)} %wq_ref.1, bf16[32,128]{1,0:T(8,128)(2,1)} %wk_ref.1, bf16[32,128]{1,0:T(8,128)(2,1)} %wv_ref.1, ...), custom_call_target="tpu_custom_call" | custom-call | flops 16777216 | bytes 1048576 | tf_op jit(solution)/shard_map/gather/pallas_call | solution.py:39
  34.1 1.1 project.1
  35.3 48.8 %attend.1 = (bf16[8,128,384]{2,1,0:T(8,128)(2,1)S(1)}, bf16[8,384,128]{2,1,0:T(8,128)(2,1)S(1)}, bf16[8,128,384]{2,1,0:T(8,128)(2,1)S(1)}, bf16[16,128]{1,0:T(8,...) custom-call(bf16[128,384]{1,0:T(8,128)(2,1)S(1)} %get-tuple-element.24.q_ref,, ...), custom_call_target="tpu_custom_call" | custom-call | flops 16777216 | bytes 1048576 | tf_op jit(solution)/shard_map/attend/pallas_call | solution.py:39
  84.1 0.0 copy-start
  84.1 0.0 copy-start.1
  84.1 0.0 copy-start.2
  84.1 157.6 %repair.1 = (f32[8,128,768]{2,1,0:T(8,128)S(1)}, f32[8,8,768]{2,1,0:T(8,128)S(1)}) custom-call(bf16[8,128,384]{2,1,0:T(8,128)(2,1)S(1)} %get-tuple-element.29.q_all, bf16[8,384,128]{2,1,0:T(8,128)(2,1)S(1)} %get-tuple-element.30.k_all, bf16[8,128,384]{2,1,0:T(8,128)(2,1)S(1)} %get-tuple-element.31.v_all, f32[8,128,768]{2,1,0:T(8,128)S(1)} %get-tuple-element.32.acc_in, ...), custom_call_target="tpu_custom_call" | custom-call | flops 16777216 | bytes 1048576 | tf_op jit(solution)/shard_map/repair/pallas_call | solution.py:39
  242.3 0.0 copy-done
  242.3 0.0 copy-done.1
  242.4 0.0 copy-done.2
  242.4 30.0 %finish.1 = bf16[48,2048]{1,0:T(8,128)(2,1)S(1)} custom-call(f32[8,128,768]{2,1,0:T(8,128)S(1)} %get-tuple-element.34.acc_ref, f32[8,8,768]{2,1,0:T(8,128)S(1)} %get-tuple-element.35.st_ref, f32[8,128]{1,0:T(8,128)S(1)} %broadcast_in_dim.8.lam_ref, f32[1,128]{1,0:T(1,128)S(1)} %bitcast.7, bf16[384,128]{1,0:T(8,128)(2,1)S(1)} %get-tuple-element.27.p_ref, ...), custom_call_target="tpu_custom_call" | custom-call | flops 16777216 | bytes 1048576 | tf_op jit(solution)/shard_map/finish/pallas_call | solution.py:39
  272.4 0.7 copy.14
  (1 shorter events, 0.0 us)
Async XLA Ops:
  84.1 158.3 %copy-start = (bf16[1,128,128]{2,1,0:T(8,128)(2,1)S(1)}, bf16[1,128,128]{2,1,0:T(8,128)(2,1)}, u32[]{:S(2)}) copy-start(bf16[1,128,128]{2,1,0:T(8,128)(2,1)} %gw_ref.1) | copy-start | bytes 98308
  84.1 158.3 %copy-start.1 = (f32[128]{0:T(128)S(1)}, f32[128]{0:T(128)}, u32[]{:S(2)}) copy-start(f32[128]{0:T(128)} %param.18) | copy-start | bytes 1540
  84.1 158.3 %copy-start.2 = (f32[128]{0:T(128)S(1)}, f32[128]{0:T(128)}, u32[]{:S(2)}) copy-start(f32[128]{0:T(128)} %param.20) | copy-start | bytes 1540
where the time goes:
time: 273 us
  Pallas kernels  270 us (99%)
    pallas_call x5, Pallas kernels, call(): pl.pallas_call(kernel, out_shape=tuple(outs), in_specs=[pl.BlockSpec(memo...  270 us

commit v1 on v0

--- a/solution.py
+++ b/solution.py
@@ -14,9 +14,8 @@
 NEG_LARGE = -1e30
 F32, BF16 = jnp.float32, jnp.bfloat16
 RIM = 16
-DEPTH = 256
-LEAD = 3
-PARTS, EARLY = 8, 6
+LEAD = 1
+PARTS = 8
 
 
 def grid_of(sp):
@@ -79,15 +78,29 @@
             ref, ref, self.ssem.at[d, sub, k], self.rsem.at[d, sub, k], self.dev((self.me + sign) % self.n)
         )
 
-    def step(self, k, subs=None, landed=None):
-        for sub in subs if subs is not None else range(self.subs):
+    def step(self, k):
+        for sub in range(self.subs):
             for d in range(2):
                 if k > 0 and k - 1 < hops(self.n, d, sub):
                     self.copy(d, sub, k - 1).wait_recv()
-                    if landed is not None:
-                        landed((self.me + (k if d else -k)) % self.n, sub)
                 if k < hops(self.n, d, sub):
                     self.copy(d, sub, k).start()
+
+    def open(self):
+        for far in range(self.steps, 0, -1):
+            for sub in range(self.subs):
+                for d in range(2):
+                    if hops(self.n, d, sub) == far:
+                        self.copy(d, sub, 0).start()
+
+    def pass_on(self, k, landed, onward):
+        for sub in range(self.subs):
+            for d in range(2):
+                if k - 1 < hops(self.n, d, sub) and (k < hops(self.n, d, sub)) == onward:
+                    self.copy(d, sub, k - 1).wait_recv()
+                    if onward:
+                        self.copy(d, sub, k).start()
+                    landed((self.me + (k if d else -k)) % self.n, sub)
 
     def finish(self):
         for k in range(self.steps):
@@ -123,15 +136,15 @@
 
     def start(self):
         self.buf[self.t] = self.own[...]
-        self.ring.step(0)
+        self.ring.open()
         self.direct = rcopy(
             self.own, self.buf.at[self.t], self.ps.at[self.subs * self.nx], self.pr.at[self.subs * self.nx], self.partner
         )
         self.direct.start()
 
-    def step(self, k, subs):
+    def step(self, k, onward):
         if k <= self.ring.steps:
-            self.ring.step(k, subs, self.relay)
+            self.ring.pass_on(k, self.relay, onward)
 
     def finish(self):
         for copy in self.relays + [self.direct]:
@@ -220,10 +233,9 @@
     ring_b.finish()
 
 
-def project_kernel(tp, tok_ref, w_ref, qt_ref, k_ref, vt_ref, pool_ref, early, late, scaled, sq):
+def project_kernel(tp, tok_ref, w_ref, qt_ref, k_ref, vt_ref, pool_ref, wo_ref, scaled, sq):
     rows, part = qt_ref.shape[1], tok_ref.shape[2]
-    early[...] = w_ref[0 : early.shape[0], 512:]
-    late[...] = w_ref[early.shape[0] :, 512:]
+    wo_ref[...] = w_ref[:, 512:]
     sq[...] = jnp.zeros_like(sq)
     for t in range(tp):
         x = tok_ref[t, 0:rows].astype(F32)
@@ -247,9 +259,12 @@
 
 
 def attend_kernel(
-    nz, ny, nx, scale, q_ref, k_ref, v_ref, p_ref, wo_ref, q_all, k_all, v_all, halo, wo_all, acc_ref, st_ref,
-    qz_ref, sum_ref, zs, zr, ys, yr, xs, xr, ps, pr, hs, hr,
+    nz, ny, nx, scale, q_ref, k_ref, v_ref, p_ref, wo_ref, lam_ref, gain_ref, gw_ref, ps_ref, out_ref,
+    q_all, k_all, v_all, halo, wo_all, acc_ref, st_ref, qz_ref, sum_ref, mix, branch, wbuf, sbuf, wland, sland, lands,
+    zs, zr, ys, yr, xs, xr, ps, pr, hs, hr, ms, mr, ss, sr, os, or_,
 ):
+    head = p_ref.shape[1]
+    orows = out_ref.shape[0]
     s, t = lax.axis_index("sp"), lax.axis_index("tp")
     z, y = s // ny, s % ny
     sp = nz * ny
@@ -257,9 +272,11 @@
     dev_y = lambda i: (z * ny + i, t)
     rows = p_ref.shape[0]
     nxt, prv = ((s + 1) % sp, t), ((s + sp - 1) % sp, t)
-    shared = Shared(nx, wo_ref, wo_all, EARLY, wo_ref.shape[0] // EARLY, xs, xr, ps, pr)
+    shared = Shared(nx, wo_ref, wo_all, PARTS, wo_ref.shape[0] // PARTS, xs, xr, ps, pr)
+    tp = 2 * nx
+    others = [(s, (t + d) % tp) for d in range(1, tp)]
     near = [dev_z((z + 1) % nz), dev_z((z + nz - 1) % nz), dev_y((y + 1) % ny), dev_y((y + ny - 1) % ny)]
-    greet(near + [nxt, prv] + shared.peers)
+    greet(near + [nxt, prv] + others)
     q_all[y] = q_ref[...]
     k_all[z] = k_ref[...]
     v_all[z] = v_ref[...]
@@ -289,41 +306,37 @@
         qz_ref[yq, :, rows:] = jnp.where(low, zero, qt)
         acc_ref[yq] = jnp.zeros((vd, lanes), F32)
         sum_ref[yq] = jnp.zeros((8, lanes), F32)
-        few = min(128, rows)
-        source = jnp.where(yq >= y, z, jnp.maximum(z - 1, 0))
-        sc = jnp.dot(k_all[source, 0:few], qz_ref[yq], preferred_element_type=F32)
-        kpos = (source * ny + y) * rows + lax.broadcasted_iota(jnp.int32, (few, 1), 0)
-        bar = jnp.max(jnp.where(kpos <= positions(yq, 0, lanes), sc, NEG_LARGE), axis=0, keepdims=True)
-        st_ref[yq, 0:1] = bar
-        st_ref[yq, 1:2] = bar * factor
+        st_ref[yq, 0:1] = jnp.full((1, lanes), NEG_LARGE, F32)
 
     def tiles(yq, blocks, mask=None):
         keys = jnp.concatenate([k_all[b] for b in blocks], axis=0)
         vals = jnp.concatenate([v_all[b] for b in blocks], axis=1)
-        depth = rows if len(blocks) == 1 else min(DEPTH, rows)
-        work = [(at, low) for at in range(0, lanes, width) for low in range(0, keys.shape[0], depth)]
-
-        def scores(item):
-            at, low = item
-            return jnp.dot(keys[low : low + depth], qz_ref[yq, :, at : at + width], preferred_element_type=F32)
-
-        ahead = [scores(item) for item in work[:LEAD]]
-        total, gain = None, None
-        for i, (at, low) in enumerate(work):
-            sc = ahead.pop(0)
+        depth = keys.shape[0]
+        work = list(range(0, lanes, width))
+
+        def scores(at):
+            sc = jnp.dot(keys, qz_ref[yq, :, at : at + width], preferred_element_type=F32)
+            if mask is not None:
+                sc = jnp.where(mask(at), sc, NEG_LARGE)
+            return sc, jnp.max(sc, axis=0, keepdims=True)
+
+        ahead = [scores(at) for at in work[:LEAD]]
+        for i, at in enumerate(work):
+            sc, top = ahead.pop(0)
             if i + LEAD < len(work):
                 ahead.append(scores(work[i + LEAD]))
             cols = slice(at, at + width)
-            expo = jnp.exp2(sc * factor - st_ref[yq, 1:2, cols])
+            old = st_ref[yq, 0:1, cols]
+            new = jnp.maximum(old, top)
+            expo = jnp.exp2(sc * factor - new * factor)
             if mask is not None:
-                expo = jnp.where(mask(at)[low : low + depth], expo, 0.0)
+                expo = jnp.where(mask(at), expo, 0.0)
+            shrink = jnp.exp2((old - new) * factor)
+            st_ref[yq, 0:1, cols] = new
             part = jnp.sum(expo.reshape(depth // 8, 8, width), axis=0)
-            total = part if low == 0 else total + part
-            term = jnp.dot(vals[:, low : low + depth], expo.astype(BF16), preferred_element_type=F32)
-            gain = term if low == 0 else gain + term
-            if low + depth == keys.shape[0]:
-                sum_ref[yq, :, cols] += total
-                acc_ref[yq, :, cols] += gain
+            sum_ref[yq, :, cols] = sum_ref[yq, :, cols] * shrink + part
+            term = jnp.dot(vals, expo.astype(BF16), preferred_element_type=F32)
+            acc_ref[yq, :, cols] = acc_ref[yq, :, cols] * shrink + term
 
     def at_distance(j, yq):
         below = z >= j
@@ -359,12 +372,16 @@
         if first < last:
             lax.fori_loop(first, last, visit, 0)
 
-    def later_visits(j):
+    def complete(first, last):
         def visit(i, carry):
-            at_distance(j, query_block(i))
-            return carry
-
-        lax.fori_loop(0, ny, visit, 0)
+            def near(j, carry):
+                at_distance(j, query_block(i))
+                return carry
+
+            return lax.fori_loop(2, ring_z.steps + 1, near, carry)
+
+        if first < last and ring_z.steps > 1:
+            lax.fori_loop(first, last, visit, 0)
 
     begin(y)
     kpos = (z * ny + y) * rows + lax.broadcasted_iota(jnp.int32, (rows, 1), 0)
@@ -374,103 +391,22 @@
         ring_y.step(k)
     ring_z.step(1)
     here = min(ny, 2 * min(sy, 2) + 1)
-    first_visits(0, min(3, here))
+    near_end, far_end = min(3, here), max(here, ny - 2)
+    first_visits(0, near_end)
+    if sz >= 2:
+        ring_z.step(2)
     if sy >= 3:
         ring_y.step(3)
-    first_visits(3, here)
-    if sz >= 2:
-        ring_z.step(2)
+    first_visits(near_end, here)
     if sy >= 4:
         ring_y.step(4)
-    shared.step(1, range(EARLY // 2))
-    first_visits(here, ny)
-    for j in range(2, sz + 1):
-        if j < sz:
-            ring_z.step(j + 1)
-        if j + 1 == sz:
-            shared.step(1, range(EARLY // 2, EARLY))
-        later_visits(j)
-    if sz < 3:
-        shared.step(1, range(EARLY // 2, EARLY))
-    shared.step(2, range(EARLY))
-    for b in range(ny):
-        st_ref[b, 1:2] = jnp.sum(sum_ref[b], axis=0, keepdims=True)
-    hcopy.wait_recv()
-    hcopy.wait_send()
-    ring_z.finish()
-    ring_y.finish()
-    shared.finish()
-
-
-def repair_kernel(ny, scale, q_all, k_all, v_all, acc_in, st_in, acc_ref, st_ref, qz_ref):
-    s = lax.axis_index("sp")
-    z, y = s // ny, s % ny
-    rows = q_all.shape[2]
-    half = q_all.shape[1] // 2
-    lanes = 2 * rows
-    factor = scale / math.log(2.0)
-    calm = jnp.max(st_in[:, 1:2]) < 2.0**80
-
-    @pl.when(calm)
-    def _():
-        acc_ref[...] = acc_in[...]
-        st_ref[:, 0:2] = st_in[:, 0:2]
-
-    @pl.when(jnp.logical_not(calm))
-    def _():
-        def slow(yq, carry):
-            qt = q_all[yq]
-            low = lax.broadcasted_iota(jnp.int32, qt.shape, 0) < half
-            zero = jnp.zeros_like(qt)
-            qz_ref[:, 0:rows] = jnp.where(low, qt, zero)
-            qz_ref[:, rows:] = jnp.where(low, zero, qt)
-            acc_ref[yq] = jnp.zeros((acc_ref.shape[1], lanes), F32)
-            st_ref[yq, 0:1] = jnp.full((1, lanes), NEG_LARGE, F32)
-            st_ref[yq, 1:2] = jnp.zeros((1, lanes), F32)
-
-            def block(b, carry):
-                kpos = (b * ny + y) * rows + lax.broadcasted_iota(jnp.int32, (rows, 1), 0)
-
-                def group(g, carry):
-                    at = pl.multiple_of(g * 128, 128)
-                    cols = pl.ds(at, 128)
-                    lane = lax.broadcasted_iota(jnp.int32, (1, 128), 1) + at
-                    qpos = jnp.where(lane >= rows, lane - rows, lane) + (z * ny + yq) * rows
-                    allowed = kpos <= qpos
-                    sc = jnp.dot(k_all[b], qz_ref[:, cols], preferred_element_type=F32)
-                    sc = jnp.where(allowed, sc, NEG_LARGE)
-                    old = st_ref[yq, 0:1, cols]
-                    new = jnp.maximum(old, jnp.max(sc, axis=0, keepdims=True))
-                    expo = jnp.where(allowed, jnp.exp2((sc - new) * factor), 0.0)
-                    shrink = jnp.exp2((old - new) * factor)
-                    st_ref[yq, 0:1, cols] = new
-                    st_ref[yq, 1:2, cols] = st_ref[yq, 1:2, cols] * shrink + jnp.sum(expo, axis=0, keepdims=True)
-                    acc_ref[yq, :, cols] = acc_ref[yq, :, cols] * shrink + jnp.dot(
-                        v_all[b], expo.astype(BF16), preferred_element_type=F32
-                    )
-                    return carry
-
-                return lax.fori_loop(0, lanes // 128, group, carry)
-
-            return lax.fori_loop(0, z + 1, block, carry)
-
-        lax.fori_loop(0, ny, slow, 0)
-
-
-def finish_kernel(
-    ny, nx, scale, acc_ref, st_ref, lam_ref, gain_ref, p_ref, halo, gw_ref, ps_ref, wo_ref, late_ref, out_ref,
-    mix, branch, wo_late, wbuf, sbuf, wland, sland, lands, ws, wr, ss, sr, xs, xr, ps, pr, os, or_,
-):
-    s, t = lax.axis_index("sp"), lax.axis_index("tp")
-    z, y = s // ny, s % ny
-    tp = 2 * nx
-    rows, head = p_ref.shape
-    orows = out_ref.shape[0]
-    factor = scale / math.log(2.0)
-    dev = lambda i: (z * ny + i % ny, t)
-    shared = Shared(nx, late_ref, wo_late, PARTS - EARLY, late_ref.shape[0] // (PARTS - EARLY), xs, xr, ps, pr)
-    others = [(s, (t + d) % tp) for d in range(1, tp)]
-    greet([dev(y + 1), dev(y + ny - 1)] + others)
+    first_visits(here, far_end)
+    if sz >= 3:
+        ring_z.step(3)
+    shared.step(1, True)
+    first_visits(far_end, ny)
+    if sz >= 4:
+        ring_z.step(4)
 
     def pooled():
         here = p_ref[...].astype(F32)
@@ -488,7 +424,7 @@
 
     def own(block, m):
         cols = slice(m * rows, (m + 1) * rows)
-        return acc_ref[block, :, cols], st_ref[block, 0:1, cols], st_ref[block, 1:2, cols]
+        return acc_ref[block, :, cols], st_ref[block, 0:1, cols], jnp.sum(sum_ref[block, :, cols], axis=0, keepdims=True)
 
     def joined(a, b):
         top = jnp.maximum(a[1], b[1])
@@ -499,13 +435,16 @@
         return wland[d, m, k].astype(F32), sland[d, m, k, 0:1], sland[d, m, k, 1:2]
 
     def copies(d, m, k):
-        to = dev(y + (1 if d == 0 else ny - 1))
+        to = dev_y((y + (1 if d == 0 else ny - 1)) % ny)
         return [
-            rcopy(wbuf.at[d, m, k], wland.at[d, m, k], ws.at[d, m, k], wr.at[d, m, k], to),
+            rcopy(wbuf.at[d, m, k], wland.at[d, m, k], ms.at[d, m, k], mr.at[d, m, k], to),
             rcopy(sbuf.at[d, m, k], sland.at[d, m, k], ss.at[d, m, k], sr.at[d, m, k], to),
         ]
 
+    done = ny
     for k in range(ny // 2):
+        complete(max(ny - 3 - 2 * k, 0), done)
+        done = max(ny - 3 - 2 * k, 0)
         for m in range(2):
             for d in range(2):
                 n = hops(ny, d, m)
@@ -524,10 +463,8 @@
                 for copy in copies(d, m, k):
                     copy.start()
         if k == 0:
-            shared.start()
+            hcopy.wait_recv()
             branch[:, head:] = pooled()
-        if k == min(2, ny // 2 - 1):
-            shared.step(1, range(PARTS - EARLY))
     for m in range(2):
         state = own(y, m)
         for d in range(2):
@@ -551,12 +488,13 @@
         outs.append(rcopy(branch.at[pl.ds(at, orows)], lands.at[t], os.at[d - 1], or_.at[d - 1], others[d - 1]))
         outs[-1].start()
     lands[t] = branch[pl.ds(pl.multiple_of(t * orows, 16), orows)]
-    shared.step(2, range(PARTS - EARLY))
+    shared.step(1, False)
+    shared.step(2, False)
     shared.finish()
     for copy in outs:
         copy.wait_recv()
     at = 0
-    for ref in (wo_ref, wo_late):
+    for ref in (wo_all,):
         step = math.gcd(512, ref.shape[1])
         for low in range(0, ref.shape[1], step):
             total = None
@@ -575,6 +513,9 @@
                 if k < hops(ny, d, m):
                     for copy in copies(d, m, k):
                         copy.wait_send()
+    hcopy.wait_send()
+    ring_z.finish()
+    ring_y.finish()
 
 
 def local(sp, tp, tokens, pre_gain, w_query, w_key, w_value, w_pool, lambdas, sub_gain, group_weight, pool_scale, w_out):
@@ -586,7 +527,6 @@
     qd = w_query.shape[1]
     whole = 3 * qd + 3 * head
     ncols = sp * w_out.shape[1]
-    early = ncols // PARTS * EARLY
     scale = 1.0 / math.sqrt(qd // 2)
     dma = pltpu.SemaphoreType.DMA
     tok_full, w_full = call(
@@ -604,63 +544,55 @@
         space=pltpu.HBM,
         name="gather",
     )
-    qt, k, vt, pool, wo_early, wo_late = call(
+    qt, k, vt, pool, wo = call(
         functools.partial(project_kernel, tp),
         (tok_full, w_full.reshape(sp * wrows, whole)),
-        (sds(qd, rows), sds(rows, qd), sds(head, rows), sds(rows, head), sds(early, 2 * head), sds(ncols - early, 2 * head)),
+        (sds(qd, rows), sds(rows, qd), sds(head, rows), sds(rows, head), sds(ncols, 2 * head)),
         [VMEM((rows, tp * part), BF16), VMEM((rows, 128), F32)],
         name="project",
-    )
-    totals = (sds(ny, head, 2 * rows, dtype=F32), sds(ny, 8, 2 * rows, dtype=F32))
-    q_all, k_all, v_all, halo, wo_all, acc, st = call(
-        functools.partial(attend_kernel, nz, ny, nx, scale),
-        (qt, k, vt, pool, wo_early),
-        (sds(ny, qd, rows), sds(nz, rows, qd), sds(nz, head, rows), sds(RIM, head), sds(tp, early, 2 * head))
-        + totals,
-        [VMEM((ny, qd, 2 * rows), BF16), VMEM((ny, 8, 2 * rows), F32)]
-        + ring_sems(nz, 2) + ring_sems(ny, 2) + shared_sems(nx, EARLY) + [dma, dma],
-        cid=1,
-        name="attend",
-    )
-    acc, st = call(
-        functools.partial(repair_kernel, ny, scale),
-        (q_all, k_all, v_all, acc, st),
-        totals,
-        [VMEM((qd, 2 * rows), BF16)],
-        name="repair",
     )
     half = ny // 2
     orows = rows // tp
     (out,) = call(
-        functools.partial(finish_kernel, ny, nx, scale),
+        functools.partial(attend_kernel, nz, ny, nx, scale),
         (
-            acc,
-            st,
+            qt,
+            k,
+            vt,
+            pool,
+            wo,
             jnp.broadcast_to(lambdas.reshape(1, 1), (8, 128)),
             sub_gain.reshape(1, head),
-            pool,
-            halo,
             group_weight,
             pool_scale.reshape(1, head),
-            wo_all,
-            wo_late,
         ),
         (sds(orows, ncols),),
         [
+            VMEM((ny, qd, rows), BF16),
+            VMEM((nz, rows, qd), BF16),
+            VMEM((nz, head, rows), BF16),
+            VMEM((RIM, head), BF16),
+            VMEM((tp, ncols, 2 * head), BF16),
+            VMEM((ny, head, 2 * rows), F32),
+            VMEM((ny, 8, 2 * rows), F32),
+            VMEM((ny, qd, 2 * rows), BF16),
+            VMEM((ny, 8, 2 * rows), F32),
             VMEM((head, rows), F32),
             VMEM((rows, 2 * head), BF16),
-            VMEM((tp, ncols - early, 2 * head), BF16),
             VMEM((2, 2, half, head, rows), BF16),
-            VMEM((2, 2, half, 8, rows), F32),
+            VMEM((2, 2, half, 2, rows), F32),
             VMEM((2, 2, half, head, rows), BF16),
-            VMEM((2, 2, half, 8, rows), F32),
+            VMEM((2, 2, half, 2, rows), F32),
             VMEM((tp, orows, 2 * head), BF16),
         ]
+        + ring_sems(nz, 2)
+        + ring_sems(ny, 2)
+        + shared_sems(nx, PARTS)
+        + [dma, dma]
         + [dma((2, 2, half))] * 4
-        + shared_sems(nx, PARTS - EARLY)
         + [dma((tp,))] * 2,
-        cid=2,
-        name="finish",
+        cid=1,
+        name="attend",
     )
     return out
 

time: 273 us -> 113 us (0.41)
  Pallas kernels: 270 us -> 108 us
    pallas_call x5 -> x3, Pallas kernels: 270 us -> 108 us  [call(): pl.pallas_call(kernel, out_shape=tuple(outs), in_specs=[pl.BlockSpec(memo...]
where the time goes in v1:
time: 113 us; the launch traced here: 111 us
  Pallas kernels  108 us (96%)
  local copies, waits for them, and re-layouts  1.95 us (2%)
    pallas_call x3, Pallas kernels, call(): pl.pallas_call(kernel, out_shape=tuple(outs), in_specs=[pl.BlockSpec(memo...  108 us

profile of v1, /device:TPU:449, one launch (start us, length us, event | category | flops | bytes accessed | tf_op | source)
XLA Modules:
  0.0 110.8 jit_solution(1555735848150347043)
XLA Ops:
  0.0 0.0 copy-start.1
  0.0 0.0 copy-start.2
  0.0 0.0 copy-start
  0.0 1.3 %reshape.14.gain_ref = bf16[1,256]{1,0:T(2,128)(2,1)} reshape(bf16[256]{0:T(256)(128)(2,1)} %param.12) | data formatting | bytes 1024 | tf_op jit(solution)/shard_map/reshape | solution.py:536
  1.3 32.9 %gather.1 = (bf16[8,400,256]{2,1,0:T(8,128)(2,1)S(1)}, bf16[8,8,2,16,768]{4,3,2,1,0:T(8,128)(2,1)S(1)}) custom-call(bf16[384,256]{1,0:T(8,128)(2,1)} %tin_ref.1, bf16[1,256]{1,0:T(2,128)(2,1)} %reshape.14.gain_ref, bf16[32,128]{1,0:T(8,128)(2,1)} %wq_ref.1, bf16[32,128]{1,0:T(8,128)(2,1)} %wk_ref.1, bf16[32,128]{1,0:T(8,128)(2,1)} %wv_ref.1, ...), custom_call_target="tpu_custom_call" | custom-call | flops 16777216 | bytes 1048576 | tf_op jit(solution)/shard_map/gather/pallas_call | solution.py:38
  34.2 1.1 %project.1 = (bf16[128,384]{1,0:T(8,128)(2,1)S(1)}, bf16[384,128]{1,0:T(8,128)(2,1)S(1)}, bf16[128,384]{1,0:T(8,128)(2,1)S(1)}, bf16[384,128]{1,0:T(8,128)(2,1)S(1)}, bf16[2048,256]{1,0:T(8,128)(2,1)S(1)}) custom-call(bf16[8,400,256]{2,1,0:T(8,128)(2,1)S(1)} %get-tuple-element.12.tok_ref, bf16[2048,768]{1,0:T(8,128)(2,1)S(1)} %bitcast.6), custom_call_target="tpu_custom_call" | custom-call | flops 16777216 | bytes 1048576 | tf_op jit(solution)/shard_map/project/pallas_call | solution.py:38
  36.0 0.0 copy-done.1
  36.0 0.0 copy-done.2
  36.0 0.0 copy-done
  36.0 74.1 %attend.1 = bf16[48,2048]{1,0:T(8,128)(2,1)S(1)} custom-call(bf16[128,384]{1,0:T(8,128)(2,1)S(1)} %get-tuple-element.14.q_ref, bf16[384,128]{1,0:T(8,128)(2,1)S(1)} %get-tuple-element.15.k_ref, bf16[128,384]{1,0:T(8,128)(2,1)S(1)} %get-tuple-element.16.v_ref, bf16[384,128]{1,0:T(8,128)(2,1)S(1)} %get-tuple-element.17.p_ref, ...), custom_call_target="tpu_custom_call" | custom-call | flops 16777216 | bytes 1048576 | tf_op jit(solution)/shard_map/attend/pallas_call | solution.py:38
  110.1 0.7 copy.14
  (1 shorter events, 0.0 us)
Async XLA Ops:
  0.0 36.0 %copy-start.1 = (f32[128]{0:T(128)S(1)}, f32[128]{0:T(128)}, u32[]{:S(2)}) copy-start(f32[128]{0:T(128)} %param.18) | copy-start | bytes 1540
  0.0 36.0 %copy-start.2 = (f32[128]{0:T(128)S(1)}, f32[128]{0:T(128)}, u32[]{:S(2)}) copy-start(f32[128]{0:T(128)} %param.20) | copy-start | bytes 1540
  0.0 36.0 %copy-start = (bf16[1,128,128]{2,1,0:T(8,128)(2,1)S(1)}, bf16[1,128,128]{2,1,0:T(8,128)(2,1)}, u32[]{:S(2)}) copy-start(bf16[1,128,128]{2,1,0:T(8,128)(2,1)} %gw_ref.1) | copy-start | bytes 98308

commit v2 on v1

--- a/solution.py
+++ b/solution.py
@@ -31,14 +31,14 @@
     return jax.ShapeDtypeStruct(shape, dtype)
 
 
-def call(kernel, ins, outs, scratch=(), cid=None, limit=40 << 20, name=None, flops=1 << 24, space=VMEM):
+def call(kernel, ins, outs, scratch=(), cid=None, limit=40 << 20, name=None, flops=1 << 24, space=()):
     params = dict(vmem_limit_bytes=limit)
     if cid is not None:
         params.update(collective_id=cid, has_side_effects=True)
     return pl.pallas_call(
         kernel,
         out_shape=tuple(outs),
-        in_specs=[pl.BlockSpec(memory_space=space)] * len(ins),
+        in_specs=[pl.BlockSpec(memory_space=one) for one in space],
         out_specs=tuple(vspec(len(outs))),
         scratch_shapes=list(scratch),
         compiler_params=pltpu.CompilerParams(**params),
@@ -159,14 +159,23 @@
     return ring_sems(nx, subs) + [dma((subs * nx + 1,)), dma((subs * nx + 1,))]
 
 
-def gather_kernel(nz, ny, nx, tin_ref, gain_ref, wq_ref, wk_ref, wv_ref, wp_ref, wo_ref, tok_full, w_full, tok_ref, w_ref, gain, ins, ts, tr, ys, yr, zs, zr, as_, ar, bs, br):
+def layer_kernel(
+    nz, ny, nx, scale, tin_ref, gain_ref, wq_ref, wk_ref, wv_ref, wp_ref, wot_ref, lam_ref, sub_ref, gw_ref, ps_ref, out_ref,
+    tok_ref, w_ref, gain, tok_full, w_full, scaled, sq, p_ref, wo_ref,
+    q_all, k_all, v_all, halo, wo_all, acc_ref, st_ref, qz_ref, sum_ref, mix, branch, wbuf, sbuf, wland, sland, lands,
+    ins, ts, tr, ys, yr, zs, zr, ga_s, ga_r, gb_s, gb_r,
+    ks, kr, qs, qr, xs, xr, ps, pr, hs, hr, ms, mr, ss, sr, os, or_,
+):
+    orows = out_ref.shape[0]
     s, t = lax.axis_index("sp"), lax.axis_index("tp")
     z, y, x, c = s // ny, s % ny, t // 2, t % 2
     half = w_ref.shape[0] // 2
-    rows = tin_ref.shape[0]
+    rows, part = tin_ref.shape
+    qd, head = wq_ref.shape[1], wv_ref.shape[1]
+    sp, tp = nz * ny, 2 * nx
     loads = [pltpu.make_async_copy(tin_ref, tok_ref.at[0:rows], ins.at[0]), pltpu.make_async_copy(gain_ref, gain, ins.at[1])]
     at = 0
-    for i, ref in enumerate((wq_ref, wk_ref, wv_ref, wp_ref, wo_ref)):
+    for i, ref in enumerate((wq_ref, wk_ref, wv_ref, wp_ref, wot_ref)):
         loads.append(pltpu.make_async_copy(ref, w_ref.at[:, at : at + ref.shape[1]], ins.at[2 + i]))
         at += ref.shape[1]
     for load in loads:
@@ -177,7 +186,11 @@
     across = [(s, ((x + d) % nx) * 2 + c) for d in range(1, nx)]
     along_y = [(z * ny + (y + d) % ny, t) for d in range(1, ny)]
     along_z = [(((z + d) % nz) * ny + y, t) for d in range(1, nz)]
-    greet([partner] + across + along_y + along_z)
+    dev_z = lambda i: (i * ny + y, t)
+    dev_y = lambda i: (z * ny + i, t)
+    nxt, prv = ((s + 1) % sp, t), ((s + sp - 1) % sp, t)
+    others = [(s, (t + d) % tp) for d in range(1, tp)]
+    greet(others + along_y + along_z + [nxt, prv])
     for i, load in enumerate(loads):
         if i != 1:
             load.wait()
@@ -202,8 +215,8 @@
     def piece_b(block, sub):
         return w_full.at[sub * (nz // 2) : (sub + 1) * (nz // 2), block, 1]
 
-    ring_a = Ring(nz, z, lambda i: (i * ny + y, t), piece_a, 2, as_, ar)
-    ring_b = Ring(ny, y, lambda i: (z * ny + i, t), piece_b, 2, bs, br)
+    ring_a = Ring(nz, z, lambda i: (i * ny + y, t), piece_a, 2, ga_s, ga_r)
+    ring_b = Ring(ny, y, lambda i: (z * ny + i, t), piece_b, 2, gb_s, gb_r)
     for copy in ysends:
         copy.wait_recv()
     ring_a.step(0)
@@ -231,58 +244,31 @@
         copy.wait_send()
     ring_a.finish()
     ring_b.finish()
-
-
-def project_kernel(tp, tok_ref, w_ref, qt_ref, k_ref, vt_ref, pool_ref, wo_ref, scaled, sq):
-    rows, part = qt_ref.shape[1], tok_ref.shape[2]
-    wo_ref[...] = w_ref[:, 512:]
+    wo_ref[...] = w_full[:, :, :, :, 512:].reshape(wo_ref.shape)
     sq[...] = jnp.zeros_like(sq)
-    for t in range(tp):
-        x = tok_ref[t, 0:rows].astype(F32)
-        gain = tok_ref[t, rows : rows + 1].astype(F32)
-        squares = x * x
-        for i in range(part // 128):
-            sq[...] += squares[:, i * 128 : (i + 1) * 128]
-        scaled[:, t * part : (t + 1) * part] = (x * gain).astype(BF16)
+    for i in range(tp):
+        values = tok_full[i, 0:rows].astype(F32)
+        weight = tok_full[i, rows : rows + 1].astype(F32)
+        squares = values * values
+        for lane in range(0, part, 128):
+            sq[...] += squares[:, lane : lane + 128]
+        scaled[:, i * part : (i + 1) * part] = (values * weight).astype(BF16)
     inverse = lax.rsqrt(jnp.sum(sq[...], axis=1, keepdims=True) / (tp * part) + EPSILON)
 
     def project(at):
-        out = jnp.dot(scaled[...], w_ref[:, at * 128 : at * 128 + 256], preferred_element_type=F32) * inverse
+        out = jnp.dot(scaled[...], w_full[:, :, :, :, at * 128 : at * 128 + 256].reshape(tp * part, 256), preferred_element_type=F32) * inverse
         return out[:, 0:128].astype(BF16), out[:, 128:256].astype(BF16)
 
     q, k = project(0)
-    qt_ref[...] = jnp.transpose(q.astype(F32)).astype(BF16)
-    k_ref[...] = k
+    q_all[y] = jnp.transpose(q.astype(F32)).astype(BF16)
+    k_all[z] = k
     v, p = project(2)
-    vt_ref[...] = jnp.transpose(v.astype(F32)).astype(BF16)
-    pool_ref[...] = p
-
-
-def attend_kernel(
-    nz, ny, nx, scale, q_ref, k_ref, v_ref, p_ref, wo_ref, lam_ref, gain_ref, gw_ref, ps_ref, out_ref,
-    q_all, k_all, v_all, halo, wo_all, acc_ref, st_ref, qz_ref, sum_ref, mix, branch, wbuf, sbuf, wland, sland, lands,
-    zs, zr, ys, yr, xs, xr, ps, pr, hs, hr, ms, mr, ss, sr, os, or_,
-):
-    head = p_ref.shape[1]
-    orows = out_ref.shape[0]
-    s, t = lax.axis_index("sp"), lax.axis_index("tp")
-    z, y = s // ny, s % ny
-    sp = nz * ny
-    dev_z = lambda i: (i * ny + y, t)
-    dev_y = lambda i: (z * ny + i, t)
-    rows = p_ref.shape[0]
-    nxt, prv = ((s + 1) % sp, t), ((s + sp - 1) % sp, t)
+    v_all[z] = jnp.transpose(v.astype(F32)).astype(BF16)
+    p_ref[...] = p
     shared = Shared(nx, wo_ref, wo_all, PARTS, wo_ref.shape[0] // PARTS, xs, xr, ps, pr)
-    tp = 2 * nx
-    others = [(s, (t + d) % tp) for d in range(1, tp)]
-    near = [dev_z((z + 1) % nz), dev_z((z + nz - 1) % nz), dev_y((y + 1) % ny), dev_y((y + ny - 1) % ny)]
-    greet(near + [nxt, prv] + others)
-    q_all[y] = q_ref[...]
-    k_all[z] = k_ref[...]
-    v_all[z] = v_ref[...]
-    half = q_ref.shape[0] // 2
-    ring_y = Ring(ny, y, dev_y, lambda b, i: q_all.at[b, i * half : (i + 1) * half], 2, ys, yr)
-    ring_z = Ring(nz, z, dev_z, lambda b, i: (k_all if i == 0 else v_all).at[b], 2, zs, zr)
+    half = qd // 2
+    ring_y = Ring(ny, y, dev_y, lambda b, i: q_all.at[b, i * half : (i + 1) * half], 2, qs, qr)
+    ring_z = Ring(nz, z, dev_z, lambda b, i: (k_all if i == 0 else v_all).at[b], 2, ks, kr)
     ring_y.step(0)
     ring_z.step(0)
     shared.start()
@@ -479,7 +465,7 @@
             mix[...] = mix[...] - lam_ref[0:1, 0:1] * state[0] / state[2]
     mixed = mix[...]
     mean = jnp.mean(mixed * mixed, axis=0, keepdims=True)
-    normed = jnp.transpose(mixed * lax.rsqrt(mean + EPSILON)) * gain_ref[...]
+    normed = jnp.transpose(mixed * lax.rsqrt(mean + EPSILON)) * sub_ref[...]
     branch[:, 0:head] = normed.astype(BF16)
 
     outs = []
@@ -529,45 +515,31 @@
     ncols = sp * w_out.shape[1]
     scale = 1.0 / math.sqrt(qd // 2)
     dma = pltpu.SemaphoreType.DMA
-    tok_full, w_full = call(
-        functools.partial(gather_kernel, nz, ny, nx),
+    half = ny // 2
+    orows = rows // tp
+    (out,) = call(
+        functools.partial(layer_kernel, nz, ny, nx, scale),
         [
             pltpu.with_memory_space_constraint(a, pltpu.HBM)
             for a in (tokens, pre_gain.reshape(1, part), w_query, w_key, w_value, w_pool, w_out.T)
-        ],
-        (sds(tp, rows + 16, part), sds(nz, ny, 2, wrows // 2, whole)),
-        [VMEM((rows + 16, part), BF16), VMEM((wrows, whole), BF16), VMEM((1, part), BF16), dma((7,))]
-        + [dma((2 * nx,)), dma((2 * nx,)), dma((ny,)), dma((ny,)), dma((nz,)), dma((nz,))]
-        + ring_sems(nz, 2)
-        + ring_sems(ny, 2),
-        cid=0,
-        space=pltpu.HBM,
-        name="gather",
-    )
-    qt, k, vt, pool, wo = call(
-        functools.partial(project_kernel, tp),
-        (tok_full, w_full.reshape(sp * wrows, whole)),
-        (sds(qd, rows), sds(rows, qd), sds(head, rows), sds(rows, head), sds(ncols, 2 * head)),
-        [VMEM((rows, tp * part), BF16), VMEM((rows, 128), F32)],
-        name="project",
-    )
-    half = ny // 2
-    orows = rows // tp
-    (out,) = call(
-        functools.partial(attend_kernel, nz, ny, nx, scale),
-        (
-            qt,
-            k,
-            vt,
-            pool,
-            wo,
+        ]
+        + [
             jnp.broadcast_to(lambdas.reshape(1, 1), (8, 128)),
             sub_gain.reshape(1, head),
             group_weight,
             pool_scale.reshape(1, head),
-        ),
+        ],
         (sds(orows, ncols),),
         [
+            VMEM((rows + 16, part), BF16),
+            VMEM((wrows, whole), BF16),
+            VMEM((1, part), BF16),
+            VMEM((tp, rows + 16, part), BF16),
+            VMEM((nz, ny, 2, wrows // 2, whole), BF16),
+            VMEM((rows, tp * part), BF16),
+            VMEM((rows, 128), F32),
+            VMEM((rows, head), BF16),
+            VMEM((ncols, 2 * head), BF16),
             VMEM((ny, qd, rows), BF16),
             VMEM((nz, rows, qd), BF16),
             VMEM((nz, head, rows), BF16),
@@ -585,14 +557,18 @@
             VMEM((2, 2, half, 2, rows), F32),
             VMEM((tp, orows, 2 * head), BF16),
         ]
+        + [dma((7,)), dma((2 * nx,)), dma((2 * nx,)), dma((ny,)), dma((ny,)), dma((nz,)), dma((nz,))]
+        + ring_sems(nz, 2)
+        + ring_sems(ny, 2)
         + ring_sems(nz, 2)
         + ring_sems(ny, 2)
         + shared_sems(nx, PARTS)
         + [dma, dma]
         + [dma((2, 2, half))] * 4
         + [dma((tp,))] * 2,
-        cid=1,
-        name="attend",
+        cid=0,
+        space=[pltpu.HBM] * 7 + [VMEM] * 4,
+        name="layer",
     )
     return out
 

time: 113 us -> 109 us (0.965); the launches traced: 111 us -> 108 us
  Pallas kernels: 108 us -> 104 us
  local copies, waits for them, and re-layouts: 1.95 us -> 3.32 us
    pallas_call x3 -> x1, Pallas kernels: 108 us -> 104 us  [call(): pl.pallas_call(kernel, out_shape=tuple(outs), in_specs=[pl.BlockSpec(memo...]
    unnamed x7 -> x9, local copies, waits for them, and re-layouts: 0.69 us -> 2.75 us
where the time goes in v2:
time: 109 us; the launch traced here: 108 us
  Pallas kernels  104 us (95%)
  local copies, waits for them, and re-layouts  3.32 us (3%)
    pallas_call x1, Pallas kernels, call(): pl.pallas_call(kernel, out_shape=tuple(outs), in_specs=[pl.BlockSpec(memo...  104 us
    unnamed x9, local copies, waits for them, and re-layouts  2.75 us

profile of v2, /device:TPU:449, one launch (start us, length us, event | category | flops | bytes accessed | tf_op | source)
XLA Modules:
  0.0 108.1 jit_solution(11796421918564087910)
XLA Ops:
  0.7 0.0 copy-start.3
  0.7 0.6 copy-done.3
  1.3 0.6 reshape.11.gain_ref
  1.9 0.0 copy-start.1
  1.9 0.0 copy-start.2
  1.9 0.6 copy-done.1
  2.5 0.0 copy-done.2
  2.5 0.0 copy-start
  2.5 0.8 copy-done
  3.3 104.1 %layer.1 = bf16[48,2048]{1,0:T(8,128)(2,1)S(1)} custom-call(bf16[384,256]{1,0:T(8,128)(2,1)} %tin_ref.1, bf16[1,256]{1,0:T(2,128)(2,1)} %reshape.11.gain_ref, bf16[32,128]{1,0:T(8,128)(2,1)} %wq_ref.1, bf16[32,128]{1,0:T(8,128)(2,1)} %wk_ref.1, bf16[32,128]{1,0:T(8,128)(2,1)} %wv_ref.1, bf16[32,128]{1,0:T(8,128)(2,1)} %wp_ref.1, bf16[32,256]{1,0:T(8,128)(2,1)} %bitcast.7, ...), custom_call_target="tpu_custom_call" | custom-call | flops 16777216 | bytes 1048576 | tf_op jit(solution)/shard_map/layer/pallas_call | solution.py:38
  107.4 0.7 copy.14
  (1 shorter events, 0.0 us)
Async XLA Ops:
  0.7 0.7 copy-start.3
  1.9 0.7 copy-start.1
  1.9 0.7 copy-start.2
  2.5 0.8 copy-start

commit v3 on v2

--- a/solution.py
+++ b/solution.py
@@ -373,9 +373,10 @@
     kpos = (z * ny + y) * rows + lax.broadcasted_iota(jnp.int32, (rows, 1), 0)
     tiles(y, [z], lambda at: kpos <= positions(y, at, width))
     sy, sz = ring_y.steps, ring_z.steps
-    for k in range(1, min(sy, 2) + 1):
-        ring_y.step(k)
+    ring_y.step(1)
     ring_z.step(1)
+    if sy >= 2:
+        ring_y.step(2)
     here = min(ny, 2 * min(sy, 2) + 1)
     near_end, far_end = min(3, here), max(here, ny - 2)
     first_visits(0, near_end)

time: 109 us -> 107 us (0.982)
  no operation moved by 1% of the time
where the time goes in v3:
time: 107 us
  Pallas kernels  103 us (96%)
  local copies, waits for them, and re-layouts  3.32 us (3%)
    pallas_call x1, Pallas kernels, call(): pl.pallas_call(kernel, out_shape=tuple(outs), in_specs=[pl.BlockSpec(memo...  103 us
    unnamed x9, local copies, waits for them, and re-layouts  2.75 us

profile of v3, /device:TPU:449, one launch (start us, length us, event | category | flops | bytes accessed | tf_op | source)
XLA Modules:
  0.0 107.1 jit_solution(402993758493223425)
XLA Ops:
  0.7 0.0 copy-start.3
  0.7 0.6 copy-done.3
  1.3 0.6 reshape.11.gain_ref
  1.9 0.0 copy-start.1
  1.9 0.0 copy-start.2
  1.9 0.6 copy-done.1
  2.5 0.0 copy-done.2
  2.5 0.0 copy-start
  2.5 0.8 copy-done
  3.3 103.1 %layer.1 = bf16[48,2048]{1,0:T(8,128)(2,1)S(1)} custom-call(bf16[384,256]{1,0:T(8,128)(2,1)} %tin_ref.1, bf16[1,256]{1,0:T(2,128)(2,1)} %reshape.11.gain_ref, bf16[32,128]{1,0:T(8,128)(2,1)} %wq_ref.1, bf16[32,128]{1,0:T(8,128)(2,1)} %wk_ref.1, bf16[32,128]{1,0:T(8,128)(2,1)} %wv_ref.1, bf16[32,128]{1,0:T(8,128)(2,1)} %wp_ref.1, bf16[32,256]{1,0:T(8,128)(2,1)} %bitcast.7, ...), custom_call_target="tpu_custom_call" | custom-call | flops 16777216 | bytes 1048576 | tf_op jit(solution)/shard_map/layer/pallas_call | solution.py:38
  106.4 0.7 copy.14
  (1 shorter events, 0.0 us)
Async XLA Ops:
  0.7 0.7 copy-start.3
  1.9 0.7 copy-start.1
  1.9 0.7 copy-start.2
  2.5 0.8 copy-start
